TPU v7x, 128 devices: a whole 4x4x4 slice. The times are simulated.
128 devices in a mesh: rep: 2 (over z_hi), fs: 32 (over z_lo, y, x), tp: 2 (over core).
Axes of the slice: x: 4, y: 4, z: 4 (z_hi: 2, z_lo: 2; z = z_hi * 2 + z_lo), core: 2. Of those that a mesh axis runs over, the one named last changes fastest.
Arguments:
- tokens: bfloat16 [64, 1024, 2048], P(('rep', 'fs'), 'tp'), may hold values from -6 to 6
- mix_gain: float32 [2048], replicated, may hold values from 0.1 to 1.9
- out_gate_w: float32 [2048, 1024], P('fs', 'tp'), may hold values from -0.125 to 0.125
- in_gate_w: float32 [2048, 1024], P('fs', 'tp'), may hold values from -0.125 to 0.125
- value_w: float32 [2048, 1024], P('fs', 'tp'), may hold values from -0.125 to 0.125
- out_gate_scale: float32 [1024], P(('tp', 'fs')), may hold values from 0.28 to 3.5
- in_gate_scale: float32 [1024], P(('tp', 'fs')), may hold values from 0.5 to 2
- value_scale: float32 [1024], P(('tp', 'fs')), may hold values from 0.5 to 2
- mix_taps: float32 [3, 1024], P(None, 'tp'), may hold values from -3.5 to 3.5
- conv_gain: float32 [1024], P('tp'), may hold values from 0.1 to 1.9
- out_proj_w: float32 [1024, 2048], P('tp', 'fs'), may hold values from -0.1875 to 0.1875
- proj_scale: float32 [2048], P('fs'), may hold values from 0.5 to 2
- ffn_gain: float32 [2048], replicated, may hold values from 0.1 to 1.9
- gate_w: float32 [2048, 2816], P('fs', 'tp'), may hold values from -0.125 to 0.125
- up_w: float32 [2048, 2816], P('fs', 'tp'), may hold values from -0.125 to 0.125
- gate_scale: float32 [2816], P(('tp', 'fs')), may hold values from 0.5 to 2
- up_scale: float32 [2816], P(('tp', 'fs')), may hold values from 0.5 to 2
- gate_taps: float32 [3, 2816], P(None, 'tp'), may hold values from -3.5 to 3.5
- up_taps: float32 [3, 2816], P(None, 'tp'), may hold values from -3.5 to 3.5
- gate_bias: float32 [2816], P('tp'), may hold values from -3 to 3
- up_bias: float32 [2816], P('tp'), may hold values from -3 to 3
- down_w: float32 [2816, 2048], P('tp', 'fs'), may hold values from -0.109375 to 0.109375
- down_scale: float32 [2048], P('fs'), may hold values from 0.5 to 2
Outputs:
- layer_out: bfloat16 [64, 1024, 2048], P(('rep', 'fs'), 'tp')
All inputs are finite; a program needn't handle non-finite values.
Results may differ from a plain program's by a relative error of at most 0.02.
Values may be sent and summed in bfloat16 or wider, within the bound.
A program may use at most 128 MiB of HBM per device.

v0:
```python
import jax
import jax.numpy as jnp
from jax import lax
from jax.sharding import PartitionSpec as P

epsilon = 1e-06


def joined_along(parts, dim):
    shape = list(parts.shape[1:])
    shape[dim] *= parts.shape[0]
    return jnp.moveaxis(parts, 0, dim).reshape(shape)


def gather_packed(arrays, axis, dims):
    ravelled = jnp.concatenate([a.reshape(-1) for a in arrays])
    lines, at, done = (lax.all_gather(ravelled, axis), 0, [])
    for a, dim in zip(arrays, dims):
        parts = lines[:, at : at + a.size].reshape(-1, *a.shape)
        done.append(joined_along(parts, dim))
        at += a.size
    return tuple(done)


def side_by_side(arrays, axis, dim, along):
    widths = [a.shape[along] for a in arrays]
    both = jnp.concatenate(arrays, axis=along)
    filled = lax.all_gather(both, axis, axis=dim, tiled=True)
    return tuple(jnp.split(filled, [sum(widths[:k]) for k in range(1, len(widths))], axis=along))


def from_everyone(shard, axis):
    size = lax.axis_size(axis)
    return lax.all_to_all(
        jnp.broadcast_to(shard[None], (size, *shard.shape)), axis, 0, 0, tiled=True
    )


def of_everyone(shard, axis):
    return from_everyone(shard, axis).sum(axis=0)


def collect(shard, axis, dim):
    return joined_along(from_everyone(shard, axis), dim)


def split_up(shard, dim, size):
    before, after = (shard.shape[:dim], shard.shape[dim + 1 :])
    return jnp.moveaxis(shard.reshape(*before, size, -1, *after), dim, 0)


def summed_on_arrival(shard, axis, dim):
    size = lax.axis_size(axis)
    parts = lax.all_to_all(split_up(shard, dim, size), axis, 0, 0, tiled=True)
    return jnp.sum(parts.astype(jnp.float32), axis=0)


def norm_rows(values, gain):
    return values * lax.rsqrt(jnp.mean(values * values, axis=-1, keepdims=True) + epsilon) * gain


def causal_taps(values, taps):
    kernel = taps.shape[0]
    length = values.shape[0]
    padded = jnp.pad(values, ((kernel - 1, 0), (0, 0)))
    total = jnp.zeros(values.shape, jnp.float32)
    for offset in range(kernel):
        total = total + taps[offset] * padded[offset : offset + length]
    return total


def column_block(left, scale_all, piece):
    return jnp.dot(left, piece, preferred_element_type=jnp.float32) * scale_all


def local(
    tokens,
    mix_gain,
    out_gate_w,
    in_gate_w,
    value_w,
    out_gate_scale,
    in_gate_scale,
    value_scale,
    mix_taps,
    conv_gain,
    out_proj_w,
    proj_scale,
    ffn_gain,
    gate_w,
    up_w,
    gate_scale,
    up_scale,
    gate_taps,
    up_taps,
    gate_bias,
    up_bias,
    down_w,
    down_scale,
):
    resid = tokens[0].astype(jnp.float32)
    normed_in = norm_rows(resid, mix_gain).astype(jnp.bfloat16)
    all_rows = lax.all_gather(normed_in, "tp", axis=0, tiled=True)
    whole_outgate, whole_ingate, whole_value, whole_gate, whole_up, whole_proj, whole_down = (
        gather_packed(
            (
                out_gate_scale,
                in_gate_scale,
                value_scale,
                gate_scale,
                up_scale,
                proj_scale,
                down_scale,
            ),
            "fs",
            (0, 0, 0, 0, 0, 0, 0),
        )
    )
    outgate_rows, ingate_rows, value_rows = side_by_side(
        (
            out_gate_w.astype(jnp.bfloat16),
            in_gate_w.astype(jnp.bfloat16),
            value_w.astype(jnp.bfloat16),
        ),
        "fs",
        0,
        1,
    )
    out_gate = (
        jnp.dot(all_rows, outgate_rows, preferred_element_type=jnp.float32) * whole_outgate
    ).astype(jnp.bfloat16)
    in_gate = (
        jnp.dot(all_rows, ingate_rows, preferred_element_type=jnp.float32) * whole_ingate
    ).astype(jnp.bfloat16)
    value_in = (
        jnp.dot(all_rows, value_rows, preferred_element_type=jnp.float32) * whole_value
    ).astype(jnp.bfloat16)
    mixed_in = in_gate.astype(jnp.float32) * value_in.astype(jnp.float32)
    conv_out = (out_gate.astype(jnp.float32) * causal_taps(mixed_in, mix_taps)).astype(jnp.bfloat16)
    conv_float = conv_out.astype(jnp.float32)
    channels = conv_float.shape[1] * lax.axis_size("tp")
    sumsq = of_everyone(jnp.sum(conv_float * conv_float, axis=1), "tp")
    mixed = (conv_float * lax.rsqrt(sumsq / channels + epsilon)[:, None] * conv_gain).astype(
        jnp.bfloat16
    )
    partial_mix = (lambda piece, start: column_block(mixed, whole_proj, piece))(
        collect(out_proj_w.astype(jnp.bfloat16), "fs", 1), jnp.int32(0)
    )
    summed = summed_on_arrival(partial_mix.astype(jnp.bfloat16), "tp", 0)
    first = (resid + summed).astype(jnp.bfloat16)
    resid_two = first.astype(jnp.float32)
    normed_ffn = norm_rows(resid_two, ffn_gain).astype(jnp.bfloat16)
    ffn_all = lax.all_gather(normed_ffn, "tp", axis=0, tiled=True)
    gate_cast = gate_w.astype(jnp.bfloat16)
    up_cast = up_w.astype(jnp.bfloat16)
    pieces = side_by_side((gate_cast, up_cast), "fs", 0, 1)
    gate_sum = jnp.dot(ffn_all, pieces[0], preferred_element_type=jnp.float32)
    up_sum = jnp.dot(ffn_all, pieces[1], preferred_element_type=jnp.float32)
    gate_pre = (gate_sum * whole_gate).astype(jnp.bfloat16)
    up_pre = (up_sum * whole_up).astype(jnp.bfloat16)
    gate_act = causal_taps(gate_pre.astype(jnp.float32), gate_taps) + gate_bias
    up_act = causal_taps(up_pre.astype(jnp.float32), up_taps) + up_bias
    hidden = (jax.nn.silu(gate_act) * up_act).astype(jnp.bfloat16)
    partial_down = column_block(
        hidden, whole_down, lax.all_gather(down_w.astype(jnp.bfloat16), "fs", axis=1, tiled=True)
    )
    summed_two = summed_on_arrival(partial_down.astype(jnp.bfloat16), "tp", 0)
    return (resid_two + summed_two).astype(jnp.bfloat16)[None]


def solution(mesh):
    placed = (
        P(("rep", "fs"), "tp", None),
        P(),
        P("fs", "tp"),
        P("fs", "tp"),
        P("fs", "tp"),
        P(("tp", "fs")),
        P(("tp", "fs")),
        P(("tp", "fs")),
        P(None, "tp"),
        P("tp"),
        P("tp", "fs"),
        P("fs"),
        P(),
        P("fs", "tp"),
        P("fs", "tp"),
        P(("tp", "fs")),
        P(("tp", "fs")),
        P(None, "tp"),
        P(None, "tp"),
        P("tp"),
        P("tp"),
        P("tp", "fs"),
        P("fs"),
    )
    return jax.shard_map(
        local, mesh=mesh, in_specs=placed, out_specs=P(("rep", "fs"), "tp", None), check_vma=False
    )
```

profile of v0, /device:TPU:1, one launch (start us, length us, event | category | flops | bytes accessed | tf_op | source)
XLA Modules:
  0.0 658.0 jit_solution(3495908413047542810)
XLA Ops:
  6.5 2.1 fusion.11
  8.8 3.5 fusion.13
  12.5 0.7 pad_maximum_fusion.1
  13.2 0.7 dynamic-slice
  15.0 135.7 %all-reduce.3 = f32[8448]{0:T(1024)S(1)} all-reduce(f32[8448]{0:T(1024)S(1)} %dynamic-update-slice), channel_id=2, replica_groups=mesh['rep'=2,'fs'=32,'tp'=2] {'fs'}, use_global_device_ids=true, to_apply=%add.3 | all-reduce | flops 8448 | bytes 67584
  151.2 25.6 %all-gather.9.cloned.1.call-done = bf16[2048,1536]{1,0:T(8,128)(2,1)} async-done(((bf16[64,1536]{1,0:T(8,128)(2,1)}), bf16[2048,1536]{1,0:T(8,128)(2,1)}) %all-gather.9.cloned.1.call-update) | async-done | bytes 6291472 | tf_op jit(solution)/shard_map/all_gather | solution.py:28
  176.8 5.4 multiply_convert_fusion.6
  182.6 2.4 convert_multiply_fusion.4
  185.0 3.1 fusion.32
  188.1 24.5 %all_to_all.21 = f32[2,1,1024]{2,1,0:T(1,128)S(1)} all-to-all(f32[2,1,1024]{2,1,0:T(1,128)S(1)} %broadcast_in_dim.4), channel_id=1, replica_groups=mesh['rep'=2,'fs'=32,'tp'=2] {'tp'}, dimensions={0} | all-to-all | bytes 16384 | tf_op jit(solution)/shard_map/all_to_all | solution.py:34
  212.7 1.6 broadcast_in_dim.5
  214.2 6.8 %all-to-all-start.1 = ((bf16[32,512,64]{1,2,0:T(8,128)(2,1)}), bf16[32,512,64]{1,2,0:T(8,128)(2,1)S(1)}, u32[]{:S(2)}, u32[]{:S(2)}) async-start(bf16[32,512,64]{1,2,0:T(8,128)(2,1)} %broadcast_in_dim.5), calls=%async_computation.1 | async-start | bytes 4194304 | tf_op jit(solution)/shard_map/all_to_all | solution.py:34
  221.2 26.7 %all-to-all-done.1 = bf16[32,512,64]{1,2,0:T(8,128)(2,1)S(1)} async-done(((bf16[32,512,64]{1,2,0:T(8,128)(2,1)}), bf16[32,512,64]{1,2,0:T(8,128)(2,1)S(1)}, u32[]{:S(2)}, u32[]{:S(2)}) %all-to-all-start.1) | async-done | bytes 2097184 | tf_op jit(solution)/shard_map/all_to_all | solution.py:34
  247.9 2.6 multiply_convert_fusion.1
  250.5 8.9 %all_to_all.22 = bf16[2,512,2048]{2,1,0:T(8,128)(2,1)S(1)} all-to-all(bf16[2,512,2048]{2,1,0:T(8,128)(2,1)S(1)} %bitcast.45), channel_id=1, replica_groups=mesh['rep'=2,'fs'=32,'tp'=2] {'tp'}, dimensions={0} | all-to-all | bytes 8388608 | tf_op jit(solution)/shard_map/all_to_all | solution.py:54
  259.4 1.0 convert_reduce_fusion.1
  260.4 0.6 copy-done.2
  261.0 0.7 fusion.16
  261.7 1.3 copy-done
  263.0 2.0 fusion.18
  265.2 0.8 pad_maximum_fusion
  266.1 0.7 convert_element_type.142
  267.2 13.0 %all-gather.11.cloned.1.call-done = bf16[1024,2048]{1,0:T(8,128)(2,1)} async-done(((bf16[512,2048]{1,0:T(8,128)(2,1)}), bf16[1024,2048]{1,0:T(8,128)(2,1)}) %all-gather.11.cloned.1.call-update) | async-done | bytes 4194320 | tf_op jit(solution)/shard_map/all_gather | solution.py:153
  280.3 155.1 %all-gather.13.cloned.1.call-done = bf16[2048,2816]{1,0:T(8,128)(2,1)} async-done(((bf16[64,2816]{1,0:T(8,128)(2,1)}), bf16[2048,2816]{1,0:T(8,128)(2,1)}) %all-gather.13.cloned.1.call-update) | async-done | bytes 11534352 | tf_op jit(solution)/shard_map/all_gather | solution.py:28
  435.4 11.8 %fusion.20 = f32[1024,1408]{1,0:T(8,128)} fusion(bf16[1024,2048]{1,0:T(8,128)(2,1)} %all-gather.11.cloned.1.call-done, bf16[2048,2816]{1,0:T(8,128)(2,1)} %all-gather.13.cloned.1.call-done, f32[1408]{0:T(1024)S(1)} %mul.270), kind=kOutput, calls=%fused_computation.28 | convolution fusion | flops 5909905408 | bytes 15734272 | tf_op jit(solution)/shard_map/dot_general | solution.py:157
  447.2 8.5 %fusion.23 = f32[1024,1408]{1,0:T(8,128)} fusion(bf16[1024,2048]{1,0:T(8,128)(2,1)S(1)} %copy-done.24, bf16[2048,2816]{1,0:T(8,128)(2,1)S(1)} %copy-done.21, f32[1408]{0:T(1024)S(1)} %mul.283), kind=kOutput, calls=%fused_computation.29 | convolution fusion | flops 5909905408 | bytes 15736832 | tf_op jit(solution)/shard_map/dot_general | solution.py:158
  455.7 139.5 %all-gather.15.cloned.1.call-done = bf16[1408,2048]{0,1:T(8,128)(2,1)} async-done(((bf16[1408,64]{0,1:T(8,128)(2,1)}), bf16[1408,2048]{0,1:T(8,128)(2,1)}) %all-gather.15.cloned.1.call-update) | async-done | bytes 5767184 | tf_op jit(solution)/shard_map/all_gather | solution.py:165
  595.2 23.3 %multiply_convert_fusion = bf16[1024,2048]{1,0:T(8,128)(2,1)} fusion(bf16[1408,2048]{0,1:T(8,128)(2,1)} %all-gather.15.cloned.1.call-done, f32[2048]{0:T(1024)S(1)} %mul.294, f32[1024,1408]{1,0:T(8,128)} %fusion.23, f32[1024,1408]{1,0:T(8,128)} %fusion.20, f32[1408]{0:T(1024)S(1)} %copy-done.25, f32[1408]{0:T(1024)S(1)} %get-tuple-element.9, ...), kind=kOutput, calls=%fused_computation.1 | convolution fusion | flops 5935726592 | bytes 21549056 | tf_op jit(solution)/shard_map/dot_general | solution.py:73
  618.5 28.2 %all_to_all.23 = bf16[2,512,2048]{2,1,0:T(8,128)(2,1)S(1)} all-to-all(bf16[2,512,2048]{2,1,0:T(8,128)(2,1)} %bitcast.44), channel_id=1, replica_groups=mesh['rep'=2,'fs'=32,'tp'=2] {'tp'}, dimensions={0} | all-to-all | bytes 8388608 | tf_op jit(solution)/shard_map/all_to_all | solution.py:54
  646.7 1.0 convert_reduce_fusion
  647.7 1.2 copy-done.1
  648.9 2.5 fusion.19
  (93 shorter events, 2.4 us)
Async XLA Ops:
  6.5 5.9 copy-start.6
  6.5 5.9 copy-start.7
  6.5 5.9 copy-start.8
  6.5 144.6 %all-gather.7.cloned.1.call-start = ((), (), s32[]{:S(2)}) async-start(), calls=%async_computation.4 | async-start | bytes 6291456 | tf_op jit(solution)/shard_map/all_gather | solution.py:103
  8.7 4.5 copy-start.28
  8.7 5.9 copy-start.14
  8.7 5.9 copy-start.15
  8.7 5.9 copy-start.16
  8.7 5.9 copy-start.17
  8.7 5.9 copy-start.18
  8.7 5.9 copy-start.19
  8.7 5.9 copy-start.20
  8.8 142.3 %copy-start.9 = (f32[512,64]{0,1:T(8,128)S(1)}, f32[512,64]{0,1:T(8,128)}, u32[]{:S(2)}) copy-start(f32[512,64]{0,1:T(8,128)} %param.33) | copy-start | bytes 393220
  8.8 142.4 %copy-start.13 = (f32[3,512]{1,0:T(4,128)S(1)}, f32[3,512]{1,0:T(4,128)}, u32[]{:S(2)}) copy-start(f32[3,512]{1,0:T(4,128)} %param.31) | copy-start | bytes 18436
  12.4 164.4 %all-gather.9.cloned.1.call-start = ((), (), s32[]{:S(2)}) async-start(), calls=%async_computation.5 | async-start | bytes 6488064 | tf_op jit(solution)/shard_map/all_gather | solution.py:28
  176.8 5.4 copy-start.22
  176.8 5.9 copy-start.23
  188.1 59.8 %copy-start.27 = (f32[512]{0:T(512)S(1)}, f32[512]{0:T(512)}, u32[]{:S(2)}) copy-start(f32[512]{0:T(512)} %param.32) | copy-start | bytes 6148
  214.2 33.7 %all-to-all-start.1 = ((bf16[32,512,64]{1,2,0:T(8,128)(2,1)}), bf16[32,512,64]{1,2,0:T(8,128)(2,1)S(1)}, u32[]{:S(2)}, u32[]{:S(2)}) async-start(bf16[32,512,64]{1,2,0:T(8,128)(2,1)} %broadcast_in_dim.5), calls=%async_computation.1 | async-start | bytes 4194304 | tf_op jit(solution)/shard_map/all_to_all | solution.py:34
  221.0 59.3 %all-gather.11.cloned.1.call-start = ((), (), s32[]{:S(2)}) async-start(), calls=%async_computation.6 | async-start | bytes 6291456 | tf_op jit(solution)/shard_map/all_gather | solution.py:153
  261.0 2.0 copy-start.12
  263.0 2.1 copy-start.3
  263.0 2.2 copy-start.4
  265.1 2.1 copy-start.10
  265.1 2.1 copy-start.11
  265.1 170.3 %all-gather.13.cloned.1.call-start = ((), (), s32[]{:S(2)}) async-start(), calls=%async_computation.7 | async-start | bytes 11894784 | tf_op jit(solution)/shard_map/all_gather | solution.py:28
  266.0 329.2 %all-gather.15.cloned.1.call-start = ((), (), s32[]{:S(2)}) async-start(), calls=%async_computation.8 | async-start | bytes 5947392 | tf_op jit(solution)/shard_map/all_gather | solution.py:165
  435.4 11.8 %copy-start.21 = (bf16[2048,2816]{1,0:T(8,128)(2,1)S(1)}, bf16[2048,2816]{1,0:T(8,128)(2,1)}, u32[]{:S(2)}) copy-start(bf16[2048,2816]{1,0:T(8,128)(2,1)} %all-gather.13.cloned.1.call-done) | copy-start | bytes 34603012
  435.4 11.8 %copy-start.24 = (bf16[1024,2048]{1,0:T(8,128)(2,1)S(1)}, bf16[1024,2048]{1,0:T(8,128)(2,1)}, u32[]{:S(2)}) copy-start(bf16[1024,2048]{1,0:T(8,128)(2,1)} %all-gather.11.cloned.1.call-done) | copy-start | bytes 12582916
  447.2 148.0 %copy-start.25 = (f32[1408]{0:T(1024)S(1)}, f32[1408]{0:T(1024)}, u32[]{:S(2)}) copy-start(f32[1408]{0:T(1024)} %param.43) | copy-start | bytes 16900
  447.2 148.0 %copy-start.26 = (f32[1408]{0:T(1024)S(1)}, f32[1408]{0:T(1024)}, u32[]{:S(2)}) copy-start(f32[1408]{0:T(1024)} %param.42) | copy-start | bytes 16900
  646.7 2.2 copy-start.1
  (3 other events, 4.6 us)
Sparse Core Ops, SparseCore 0:
  12.5 19.9 all-gather.6
  34.1 142.5 all-gather.8
  265.2 15.0 all-gather.10
  281.8 153.5 all-gather.12
  436.9 158.2 all-gather.14
where the time goes:
time: 658 us
  waiting for transfers between devices  360 us (55%)
  blocking collectives  197 us (30%)
  matrix products  57 us (9%)
  other arithmetic  15.1 us (2%)
  between operations  14.3 us (2%)
  local copies, waits for them, and re-layouts  7.36 us (1%)
  starting transfers between devices  6.92 us (1%)
    all_gather x2, waiting for transfers between devices, side_by_side(): filled = lax.all_gather(both, axis, axis=dim, tiled=True)  181 us
    all_gather x1, waiting for transfers between devices, local(): lax.all_gather(down_w.astype(jnp.bfloat16), 'fs', axis=1, tiled=True)  139 us
    unnamed x1, blocking collectives  136 us
    all_to_all x2, blocking collectives, summed_on_arrival(): parts = lax.all_to_all(split_up(shard, dim, size), axis, 0, 0, tiled=True)  37.1 us
    all_to_all x1, waiting for transfers between devices, from_everyone(): lax.all_to_all(jnp.broadcast_to(shard[None], (size, *shard.shape)), axis,...  26.7 us
    dot_general x2, matrix products, column_block(): return jnp.dot(left, piece, preferred_element_type=jnp.float32) * scale_all  25.9 us
    all_to_all x1, blocking collectives, from_everyone(): lax.all_to_all(jnp.broadcast_to(shard[None], (size, *shard.shape)), axis,...  24.5 us
  transfers between devices with their start and end apart: 6, of which 5 were waited for; matrix products, arithmetic and copies ran while one was open for 4% of the time, Pallas kernels for 0%

commit v1 on v0

--- a/solution.py
+++ b/solution.py
@@ -162,7 +162,9 @@
     up_act = causal_taps(up_pre.astype(jnp.float32), up_taps) + up_bias
     hidden = (jax.nn.silu(gate_act) * up_act).astype(jnp.bfloat16)
     partial_down = column_block(
-        hidden, whole_down, lax.all_gather(down_w.astype(jnp.bfloat16), "fs", axis=1, tiled=True)
+        hidden,
+        whole_down,
+        jnp.concatenate(lax.all_gather(down_w.astype(jnp.bfloat16), "fs"), axis=1),
     )
     summed_two = summed_on_arrival(partial_down.astype(jnp.bfloat16), "tp", 0)
     return (resid_two + summed_two).astype(jnp.bfloat16)[None]

time: 658 us -> 627 us (0.953)
  waiting for transfers between devices: 360 us -> 322 us
  local copies, waits for them, and re-layouts: 7.36 us -> 15.2 us
    all_gather x1, waiting for transfers between devices: 139 us -> 74.7 us  [local(): lax.all_gather(down_w.astype(jnp.bfloat16), 'fs')]
    all_gather x1, waiting for transfers between devices: 13 us -> 29.8 us  [local(): ffn_all = lax.all_gather(normed_ffn, 'tp', axis=0, tiled=True)]
    all_to_all x1, waiting for transfers between devices: 26.7 us -> 37.5 us  [from_everyone(): lax.all_to_all(jnp.broadcast_to(shard[None], (size, *shard.shape)), axis,...]
  transfers between devices with their start and end apart: 6 -> 6, of which waited for: 5 -> 5; matrix products, arithmetic and copies ran while one was open for 4% -> 5% of each run, Pallas kernels for 0% -> 0%
where the time goes in v1:
time: 627 us
  waiting for transfers between devices  322 us (51%)
  blocking collectives  196 us (31%)
  matrix products  57 us (9%)
  local copies, waits for them, and re-layouts  15.2 us (2%)
  other arithmetic  15.2 us (2%)
  between operations  14.1 us (2%)
  starting transfers between devices  7.21 us (1%)
    all_gather x2, waiting for transfers between devices, side_by_side(): filled = lax.all_gather(both, axis, axis=dim, tiled=True)  180 us
    unnamed x1, blocking collectives  137 us
    all_gather x1, waiting for transfers between devices, local(): lax.all_gather(down_w.astype(jnp.bfloat16), 'fs')  74.7 us
    all_to_all x1, waiting for transfers between devices, from_everyone(): lax.all_to_all(jnp.broadcast_to(shard[None], (size, *shard.shape)), axis,...  37.5 us
    all_to_all x2, blocking collectives, summed_on_arrival(): parts = lax.all_to_all(split_up(shard, dim, size), axis, 0, 0, tiled=True)  35.6 us
    all_gather x1, waiting for transfers between devices, local(): ffn_all = lax.all_gather(normed_ffn, 'tp', axis=0, tiled=True)  29.8 us
    dot_general x2, matrix products, column_block(): return jnp.dot(left, piece, preferred_element_type=jnp.float32) * scale_all  25.9 us
    all_to_all x1, blocking collectives, from_everyone(): lax.all_to_all(jnp.broadcast_to(shard[None], (size, *shard.shape)), axis,...  23.8 us
  transfers between devices with their start and end apart: 6, of which 5 were waited for; matrix products, arithmetic and copies ran while one was open for 5% of the time, Pallas kernels for 0%

profile of v1, /device:TPU:1, one launch (start us, length us, event | category | flops | bytes accessed | tf_op | source)
XLA Modules:
  0.0 626.6 jit_solution(9092395156349624490)
XLA Ops:
  6.5 2.1 fusion.11
  8.8 3.6 fusion.13
  12.6 0.7 pad_maximum_fusion.1
  13.3 0.7 convert_element_type.142
  15.6 136.8 %all-reduce.3 = f32[8448]{0:T(1024)S(1)} all-reduce(f32[8448]{0:T(1024)S(1)} %dynamic-update-slice), channel_id=2, replica_groups=mesh['rep'=2,'fs'=32,'tp'=2] {'fs'}, use_global_device_ids=true, to_apply=%add.3 | all-reduce | flops 8448 | bytes 67584
  152.9 24.5 %all-gather.10.cloned.1.call-done = bf16[2048,1536]{1,0:T(8,128)(2,1)} async-done(((bf16[64,1536]{1,0:T(8,128)(2,1)}), bf16[2048,1536]{1,0:T(8,128)(2,1)}) %all-gather.10.cloned.1.call-update) | async-done | bytes 6291472 | tf_op jit(solution)/shard_map/all_gather | solution.py:28
  177.4 5.4 multiply_convert_fusion.6
  183.3 2.4 convert_multiply_fusion.4
  185.7 3.1 fusion.32
  188.8 23.8 %all_to_all.21 = f32[2,1,1024]{2,1,0:T(1,128)S(1)} all-to-all(f32[2,1,1024]{2,1,0:T(1,128)S(1)} %broadcast_in_dim.4), channel_id=1, replica_groups=mesh['rep'=2,'fs'=32,'tp'=2] {'tp'}, dimensions={0} | all-to-all | bytes 16384 | tf_op jit(solution)/shard_map/all_to_all | solution.py:34
  212.5 1.6 broadcast_in_dim.5
  214.1 6.9 %all-to-all-start.1 = ((bf16[32,512,64]{1,2,0:T(8,128)(2,1)}), bf16[32,512,64]{1,2,0:T(8,128)(2,1)S(1)}, u32[]{:S(2)}, u32[]{:S(2)}) async-start(bf16[32,512,64]{1,2,0:T(8,128)(2,1)} %broadcast_in_dim.5), calls=%async_computation.1 | async-start | bytes 4194304 | tf_op jit(solution)/shard_map/all_to_all | solution.py:34
  221.2 37.5 %all-to-all-done.1 = bf16[32,512,64]{1,2,0:T(8,128)(2,1)S(1)} async-done(((bf16[32,512,64]{1,2,0:T(8,128)(2,1)}), bf16[32,512,64]{1,2,0:T(8,128)(2,1)S(1)}, u32[]{:S(2)}, u32[]{:S(2)}) %all-to-all-start.1) | async-done | bytes 2097184 | tf_op jit(solution)/shard_map/all_to_all | solution.py:34
  258.7 2.6 multiply_convert_fusion.1
  261.3 7.5 %all_to_all.22 = bf16[2,512,2048]{2,1,0:T(8,128)(2,1)S(1)} all-to-all(bf16[2,512,2048]{2,1,0:T(8,128)(2,1)S(1)} %bitcast.55), channel_id=1, replica_groups=mesh['rep'=2,'fs'=32,'tp'=2] {'tp'}, dimensions={0} | all-to-all | bytes 8388608 | tf_op jit(solution)/shard_map/all_to_all | solution.py:54
  268.8 1.0 convert_reduce_fusion.1
  270.4 0.7 fusion.16
  271.0 1.3 copy-done
  272.4 2.0 fusion.18
  274.8 0.8 pad_maximum_fusion
  276.0 74.7 %all-gather.16.cloned.1.call-done = bf16[45056,64]{0,1:T(8,128)(2,1)} async-done(((bf16[1408,64]{0,1:T(8,128)(2,1)}), bf16[45056,64]{0,1:T(8,128)(2,1)}) %all-gather.16.cloned.1.call-update) | async-done | bytes 5767184 | tf_op jit(solution)/shard_map/all_gather | solution.py:167
  350.7 3.5 copy.42
  354.2 4.4 copy.38
  358.7 29.8 %all-gather.12.cloned.1.call-done = bf16[1024,2048]{1,0:T(8,128)(2,1)} async-done(((bf16[512,2048]{1,0:T(8,128)(2,1)}), bf16[1024,2048]{1,0:T(8,128)(2,1)}) %all-gather.12.cloned.1.call-update) | async-done | bytes 4194320 | tf_op jit(solution)/shard_map/all_gather | solution.py:153
  388.5 155.1 %all-gather.14.cloned.1.call-done = bf16[2048,2816]{1,0:T(8,128)(2,1)} async-done(((bf16[64,2816]{1,0:T(8,128)(2,1)}), bf16[2048,2816]{1,0:T(8,128)(2,1)}) %all-gather.14.cloned.1.call-update) | async-done | bytes 11534352 | tf_op jit(solution)/shard_map/all_gather | solution.py:28
  543.5 11.8 %fusion.20 = f32[1024,1408]{1,0:T(8,128)} fusion(bf16[1024,2048]{1,0:T(8,128)(2,1)} %all-gather.12.cloned.1.call-done, bf16[2048,2816]{1,0:T(8,128)(2,1)} %all-gather.14.cloned.1.call-done, f32[1408]{0:T(1024)S(1)} %mul.270), kind=kOutput, calls=%fused_computation.28 | convolution fusion | flops 5909905408 | bytes 15734272 | tf_op jit(solution)/shard_map/dot_general | solution.py:157
  555.4 8.5 %fusion.23 = f32[1024,1408]{1,0:T(8,128)} fusion(bf16[1024,2048]{1,0:T(8,128)(2,1)S(1)} %copy-done.24, bf16[2048,2816]{1,0:T(8,128)(2,1)S(1)} %copy-done.21, f32[1408]{0:T(1024)S(1)} %mul.283), kind=kOutput, calls=%fused_computation.29 | convolution fusion | flops 5909905408 | bytes 15736832 | tf_op jit(solution)/shard_map/dot_general | solution.py:158
  563.9 23.3 %multiply_convert_fusion = bf16[1024,2048]{1,0:T(8,128)(2,1)} fusion(bf16[1408,2048]{0,1:T(8,128)(2,1)} %bitcast.53, f32[2048]{0:T(1024)S(1)} %mul.294, f32[1024,1408]{1,0:T(8,128)} %fusion.23, f32[1024,1408]{1,0:T(8,128)} %fusion.20, f32[1408]{0:T(1024)S(1)} %copy-done.25, f32[1408]{0:T(1024)S(1)} %get-tuple-element.9, f32[1408]{0:T(1024)S(1)} %get-tuple-element.10, ...), kind=kOutput, calls=%fused_computation.1 | convolution fusion | flops 5935726592 | bytes 21549056 | tf_op jit(solution)/shard_map/dot_general | solution.py:73
  587.2 28.2 %all_to_all.23 = bf16[2,512,2048]{2,1,0:T(8,128)(2,1)S(1)} all-to-all(bf16[2,512,2048]{2,1,0:T(8,128)(2,1)} %bitcast.54), channel_id=1, replica_groups=mesh['rep'=2,'fs'=32,'tp'=2] {'tp'}, dimensions={0} | all-to-all | bytes 8388608 | tf_op jit(solution)/shard_map/all_to_all | solution.py:54
  615.4 1.0 convert_reduce_fusion
  616.4 1.2 copy-done.1
  617.6 2.5 fusion.19
  (95 shorter events, 3.8 us)
Async XLA Ops:
  6.5 5.9 copy-start.6
  6.5 6.0 copy-start.7
  6.5 6.0 copy-start.8
  6.5 146.4 %all-gather.8.cloned.1.call-start = ((), (), s32[]{:S(2)}) async-start(), calls=%async_computation.4 | async-start | bytes 6291456 | tf_op jit(solution)/shard_map/all_gather | solution.py:103
  8.7 4.7 copy-start.3
  8.7 5.4 copy-start.28
  8.7 6.5 %copy-start.14 = (f32[16]{0:T(128)S(1)}, f32[16]{0:T(128)}, u32[]{:S(2)}) copy-start(f32[16]{0:T(128)} %param.28) | copy-start | bytes 196
  8.7 6.5 %copy-start.15 = (f32[16]{0:T(128)S(1)}, f32[16]{0:T(128)}, u32[]{:S(2)}) copy-start(f32[16]{0:T(128)} %param.29) | copy-start | bytes 196
  8.7 6.5 %copy-start.16 = (f32[16]{0:T(128)S(1)}, f32[16]{0:T(128)}, u32[]{:S(2)}) copy-start(f32[16]{0:T(128)} %param.30) | copy-start | bytes 196
  8.7 6.5 %copy-start.17 = (f32[44]{0:T(128)S(1)}, f32[44]{0:T(128)}, u32[]{:S(2)}) copy-start(f32[44]{0:T(128)} %param.38) | copy-start | bytes 532
  8.7 6.5 %copy-start.18 = (f32[44]{0:T(128)S(1)}, f32[44]{0:T(128)}, u32[]{:S(2)}) copy-start(f32[44]{0:T(128)} %param.39) | copy-start | bytes 532
  8.7 6.5 %copy-start.19 = (f32[64]{0:T(128)S(1)}, f32[64]{0:T(128)}, u32[]{:S(2)}) copy-start(f32[64]{0:T(128)} %param.34) | copy-start | bytes 772
  8.8 6.5 %copy-start.20 = (f32[64]{0:T(128)S(1)}, f32[64]{0:T(128)}, u32[]{:S(2)}) copy-start(f32[64]{0:T(128)} %param.45) | copy-start | bytes 772
  8.8 144.1 %copy-start.9 = (f32[512,64]{0,1:T(8,128)S(1)}, f32[512,64]{0,1:T(8,128)}, u32[]{:S(2)}) copy-start(f32[512,64]{0,1:T(8,128)} %param.33) | copy-start | bytes 393220
  8.8 144.1 %copy-start.13 = (f32[3,512]{1,0:T(4,128)S(1)}, f32[3,512]{1,0:T(4,128)}, u32[]{:S(2)}) copy-start(f32[3,512]{1,0:T(4,128)} %param.31) | copy-start | bytes 18436
  12.4 165.0 %all-gather.10.cloned.1.call-start = ((), (), s32[]{:S(2)}) async-start(), calls=%async_computation.5 | async-start | bytes 6488064 | tf_op jit(solution)/shard_map/all_gather | solution.py:28
  13.3 337.4 %all-gather.16.cloned.1.call-start = ((), (), s32[]{:S(2)}) async-start(), calls=%async_computation.8 | async-start | bytes 5947392 | tf_op jit(solution)/shard_map/all_gather | solution.py:167
  177.4 5.4 copy-start.22
  177.4 5.9 copy-start.23
  188.7 70.0 %copy-start.27 = (f32[512]{0:T(512)S(1)}, f32[512]{0:T(512)}, u32[]{:S(2)}) copy-start(f32[512]{0:T(512)} %param.32) | copy-start | bytes 6148
  214.1 44.6 %all-to-all-start.1 = ((bf16[32,512,64]{1,2,0:T(8,128)(2,1)}), bf16[32,512,64]{1,2,0:T(8,128)(2,1)S(1)}, u32[]{:S(2)}, u32[]{:S(2)}) async-start(bf16[32,512,64]{1,2,0:T(8,128)(2,1)} %broadcast_in_dim.5), calls=%async_computation.1 | async-start | bytes 4194304 | tf_op jit(solution)/shard_map/all_to_all | solution.py:34
  220.9 167.5 %all-gather.12.cloned.1.call-start = ((), (), s32[]{:S(2)}) async-start(), calls=%async_computation.6 | async-start | bytes 6291456 | tf_op jit(solution)/shard_map/all_gather | solution.py:153
  270.4 2.0 copy-start
  270.4 2.0 copy-start.12
  272.4 2.3 copy-start.4
  272.4 2.3 copy-start.5
  274.4 269.1 %all-gather.14.cloned.1.call-start = ((), (), s32[]{:S(2)}) async-start(), calls=%async_computation.7 | async-start | bytes 11894784 | tf_op jit(solution)/shard_map/all_gather | solution.py:28
  543.5 11.8 %copy-start.21 = (bf16[2048,2816]{1,0:T(8,128)(2,1)S(1)}, bf16[2048,2816]{1,0:T(8,128)(2,1)}, u32[]{:S(2)}) copy-start(bf16[2048,2816]{1,0:T(8,128)(2,1)} %all-gather.14.cloned.1.call-done) | copy-start | bytes 34603012
  543.5 11.8 %copy-start.24 = (bf16[1024,2048]{1,0:T(8,128)(2,1)S(1)}, bf16[1024,2048]{1,0:T(8,128)(2,1)}, u32[]{:S(2)}) copy-start(bf16[1024,2048]{1,0:T(8,128)(2,1)} %all-gather.12.cloned.1.call-done) | copy-start | bytes 12582916
  555.4 8.5 %copy-start.25 = (f32[1408]{0:T(1024)S(1)}, f32[1408]{0:T(1024)}, u32[]{:S(2)}) copy-start(f32[1408]{0:T(1024)} %param.43) | copy-start | bytes 16900
  555.4 8.5 %copy-start.26 = (f32[1408]{0:T(1024)S(1)}, f32[1408]{0:T(1024)}, u32[]{:S(2)}) copy-start(f32[1408]{0:T(1024)} %param.42) | copy-start | bytes 16900
  615.4 2.2 copy-start.1
  (3 other events, 4.5 us)
Sparse Core Ops, SparseCore 0:
  12.5 19.9 all-gather.7
  34.2 143.1 all-gather.9
  179.1 171.5 all-gather.15
  352.2 36.2 all-gather.11
  389.9 153.5 all-gather.13
